TPU v7x, 32 devices: a whole 2x2x4 slice. The times are simulated.
32 devices in a mesh: ep: 8 (over z, x), tp: 4 (over y, core).
Axes of the slice: x: 2, y: 2, z: 4, core: 2. Of those that a mesh axis runs over, the one named last changes fastest.
Arguments:
- mixer_input: bfloat16 [4096, 2048], P('ep'), may hold values from -6 to 6
- mixer_gain: float32 [2048], replicated, may hold values from 0.1 to 1.9
- query_weight: bfloat16 [2048, 1024], P(None, 'tp'), may hold values from -0.125 to 0.125
- key_weight: bfloat16 [2048, 1024], P(None, 'tp'), may hold values from -0.125 to 0.125
- value_weight: bfloat16 [2048, 1024], P(None, 'tp'), may hold values from -0.125 to 0.125
- gate_weight: bfloat16 [2048, 1024], P(None, 'tp'), may hold values from -0.125 to 0.125
- head_gain: float32 [1024], P('tp'), may hold values from 0.1 to 1.9
- output_weight: bfloat16 [1024, 2048], P('tp'), may hold values from -0.1875 to 0.1875
- log_decay: float32 [4096, 8], P('ep', 'tp'), may hold values from -1 to 0, as said below
- expert_input: bfloat16 [4096, 2048], P(('ep', 'tp')), may hold values from -6 to 6
- expert_gain: float32 [2048], replicated, may hold values from 0.1 to 1.9
- routes: int32 [4096, 2], P(('ep', 'tp')), may hold values from 0 to 7, all different within a row; in each aligned block of 128 rows (0 to 127, 128 to 255, ...) at most 48 rows name the same one
- route_weight: float32 [4096, 2], P(('ep', 'tp')), may hold values from 0.1 to 1
- expert_gate: bfloat16 [8, 2048, 1024], P('ep', None, 'tp'), may hold values from -0.125 to 0.125
- expert_up: bfloat16 [8, 2048, 1024], P('ep', None, 'tp'), may hold values from -0.125 to 0.125
- expert_down: bfloat16 [8, 1024, 2048], P('ep', 'tp'), may hold values from -0.1875 to 0.1875
Outputs:
- mixer_output: bfloat16 [4096, 2048], P(('ep', 'tp'))
- expert_output: bfloat16 [4096, 2048], P(('ep', 'tp'))
Inputs may be any that keep to these rules, and one draw needn't show every extreme that they name: `routes`: each row names 2 different experts. Among the rows of one device no expert is named more than 48 times, and in every draw the rows of some device name some expert exactly 48 times. `log_decay`: negative values.
All inputs are finite; a program needn't handle non-finite values.
Results may differ from a plain program's by a relative error of at most 0.025.
Values may be sent and summed in bfloat16 or wider, within the bound.
No kernel may reach another device: no remote copies, remote signals or barrier semaphores. Data moves between devices by JAX's collectives and lax.ppermute only.
A program may use at most 128 MiB of HBM per device.

v0:
```python
import functools

import jax
import jax.numpy as jnp
from jax import lax
from jax.experimental import pallas as pl
from jax.experimental.pallas import tpu as pltpu
from jax.sharding import PartitionSpec as P


BLOCK = 128
EPS = 1e-06
HIGH = lax.Precision.HIGHEST
PAD = 16
F32 = jnp.float32
BF16 = jnp.bfloat16


def dot(a, b, contract=((1,), (0,)), precision=None):
    return lax.dot_general(
        a, b, (contract, ((), ())), preferred_element_type=F32, precision=precision
    )


def normed_rows(values, gain):
    floats = values.astype(F32)
    scale = lax.rsqrt(jnp.mean(floats * floats, axis=-1, keepdims=True) + EPS)
    return (floats * scale * gain).astype(BF16)


def silu(v):
    return v / (1.0 + jnp.exp(-v))


def retain_kernel(
    x_ref,
    gain_ref,
    wq_ref,
    wk_ref,
    wv_ref,
    wg_ref,
    cos_ref,
    sin_ref,
    ldt_ref,
    ret_ref,
    qd_ref,
    gate_ref,
    pkg_ref,
    normed_ref,
    *,
    heads,
    head_dim,
):
    rows = x_ref.shape[0]
    blocks = rows // BLOCK
    for b in range(blocks):
        part = slice(b * BLOCK, (b + 1) * BLOCK)
        normed_ref[part, :] = normed_rows(x_ref[part, :], gain_ref[...])
    normed = normed_ref[...]
    q_all = dot(normed, wq_ref[...]).astype(BF16)
    k_all = dot(normed, wk_ref[...]).astype(BF16)
    v_all = dot(normed, wv_ref[...]).astype(BF16)
    gate_ref[...] = dot(normed, wg_ref[...]).astype(BF16)
    row_ids = lax.broadcasted_iota(jnp.int32, (BLOCK, BLOCK), 0)
    col_ids = lax.broadcasted_iota(jnp.int32, (BLOCK, BLOCK), 1)
    lower = col_ids <= row_ids
    tri = lower.astype(F32)
    tri_t = (row_ids <= col_ids).astype(F32)
    states = [jnp.zeros((head_dim, head_dim), F32) for _ in range(heads)]
    base = [jnp.zeros((1, 1), F32) for _ in range(heads)]
    for b in range(blocks):
        part = slice(b * BLOCK, (b + 1) * BLOCK)
        c_cols = dot(tri, ldt_ref[:, part], ((1,), (1,)), precision=HIGH)
        c_rows = dot(ldt_ref[:, part], tri_t, precision=HIGH)
        cosine, sine = cos_ref[part, :], sin_ref[part, :]
        for h in range(heads):
            lanes = slice(h * head_dim, (h + 1) * head_dim)
            c_col = c_cols[:, h : h + 1]
            c_row = c_rows[h : h + 1, :]
            total = c_row[:, BLOCK - 1 : BLOCK]
            q = q_all[part, lanes].astype(F32)
            k = k_all[part, lanes].astype(F32)
            v = v_all[part, lanes]
            q = (q * cosine + pltpu.roll(q, head_dim // 2, 1) * sine).astype(BF16)
            k = (k * cosine + pltpu.roll(k, head_dim // 2, 1) * sine) * head_dim ** (-0.5)
            k = k.astype(BF16)
            decays = jnp.where(lower, jnp.exp(jnp.where(lower, c_col - c_row, 0.0)), 0.0)
            weights = (dot(q, k, ((1,), (1,))) * decays).astype(BF16)
            qf = q.astype(F32)
            inner = dot(weights, v)
            if b:
                inner = inner + dot((qf * jnp.exp(c_col)).astype(BF16), states[h].astype(BF16))
            ret_ref[part, lanes] = inner
            qd_ref[part, lanes] = (qf * jnp.exp(c_col + base[h])).astype(BF16)
            scaled = (k.astype(F32) * jnp.exp(total - c_col)).astype(BF16)
            update = dot(scaled, v, ((0,), (0,)))
            states[h] = jnp.exp(total) * states[h] + update
            base[h] = base[h] + total
    span = head_dim + PAD
    peers = pkg_ref.shape[0]
    for h in range(heads):
        state = states[h].astype(BF16)
        factor = jnp.broadcast_to(jnp.exp(base[h]), (PAD, head_dim)).astype(BF16)
        pkg_ref[:, h * span : h * span + head_dim, :] = jnp.broadcast_to(
            state[None], (peers,) + state.shape
        )
        pkg_ref[:, h * span + head_dim : (h + 1) * span, :] = jnp.broadcast_to(
            factor[None], (peers,) + factor.shape
        )


def finish_kernel(index_ref, ret_ref, qd_ref, gate_ref, hgain_ref, wo_ref, pkg_ref, *refs, heads, head_dim):
    outs, hidden_ref = refs[:-1], refs[-1]
    pieces = len(outs)
    span = head_dim + PAD
    for h in range(heads):
        lanes = slice(h * head_dim, (h + 1) * head_dim)

        def turn(k, state, h=h):
            local = pkg_ref[k, h * span : h * span + head_dim, :].astype(F32)
            factor = pkg_ref[k, h * span + head_dim : (h + 1) * span, :].astype(F32)[0:1, :]
            return factor * state + local

        state = lax.fori_loop(0, index_ref[pieces], turn, jnp.zeros((head_dim, head_dim), F32))
        kept = ret_ref[:, lanes] + dot(qd_ref[:, lanes], state.astype(BF16))
        centre = jnp.mean(kept, axis=-1, keepdims=True)
        away = kept - centre
        spread = jnp.mean(away * away, axis=-1, keepdims=True)
        scaled = away * lax.rsqrt(spread + EPS) * hgain_ref[:, lanes]
        hidden_ref[:, lanes] = (scaled * silu(gate_ref[:, lanes].astype(F32))).astype(BF16)
    for j in reversed(range(pieces)):
        size = outs[j].shape[0]
        start = pl.multiple_of(index_ref[j] * size, size)
        outs[j][...] = dot(hidden_ref[pl.ds(start, size), :], wo_ref[...]).astype(BF16)


def dispatch_kernel(x_ref, gain_ref, routes_ref, weight_ref, out_ref, hi_ref, lo_ref, *, capacity):
    top, tokens = routes_ref.shape
    slots = out_ref.shape[0]
    experts = slots // capacity
    normed = normed_rows(x_ref[...], gain_ref[...])
    row_ids = lax.broadcasted_iota(jnp.int32, (tokens, tokens), 0)
    col_ids = lax.broadcasted_iota(jnp.int32, (tokens, tokens), 1)
    before = (row_ids < col_ids).astype(F32).astype(BF16)
    line = lax.broadcasted_iota(jnp.int32, (experts, tokens), 0)
    slot = lax.broadcasted_iota(jnp.int32, (slots, tokens), 0)
    routes = routes_ref[...]
    scores = weight_ref[...]
    share = scores / jnp.sum(scores, axis=0, keepdims=True)
    offset = jnp.zeros((experts, 1), F32)
    place = jnp.zeros((slots, tokens), F32)
    mix = jnp.zeros((slots, tokens), F32)
    for t in range(top):
        expert = routes[t : t + 1, :]
        onehot = (line == expert).astype(F32)
        prior = dot(onehot.astype(BF16), before) + offset
        position = jnp.sum(prior * onehot, axis=0, keepdims=True)
        target = expert * capacity + position.astype(jnp.int32)
        hit = (slot == target).astype(F32)
        place = place + hit
        mix = mix + hit * share[t : t + 1, :]
        offset = offset + jnp.sum(onehot, axis=1, keepdims=True)
    out_ref[...] = dot(place.astype(BF16), normed).astype(BF16)
    high = mix.astype(BF16)
    hi_ref[...] = high
    lo_ref[...] = (mix - high.astype(F32)).astype(BF16)


def gate_up_kernel(rows_ref, *refs, pieces):
    gates, ups = refs[:pieces], refs[pieces : 2 * pieces]
    out_ref, gacc_ref, uacc_ref = refs[2 * pieces :]
    step = pl.program_id(0)
    rows = rows_ref[...]
    width = gates[0].shape[1]

    @pl.when(step == 0)
    def _():
        gacc_ref[...] = jnp.zeros_like(gacc_ref)
        uacc_ref[...] = jnp.zeros_like(uacc_ref)

    for i in range(pieces):
        lanes = slice(i * width, (i + 1) * width)
        gacc_ref[:, lanes] += dot(rows, gates[i][...])
        uacc_ref[:, lanes] += dot(rows, ups[i][...])

    @pl.when(step == pl.num_programs(0) - 1)
    def _():
        out_ref[...] = (silu(gacc_ref[...]) * uacc_ref[...]).astype(BF16)


def gate_up(rows, gates, ups):
    count, width = rows.shape
    pieces, cols = len(gates), gates[0].shape[1]
    part = width // 4
    weight = pl.BlockSpec((part, cols), lambda i: (i, 0))
    return pl.pallas_call(
        functools.partial(gate_up_kernel, pieces=pieces),
        grid=(4,),
        in_specs=[pl.BlockSpec((count, part), lambda i: (0, i))] + [weight] * (2 * pieces),
        out_specs=pl.BlockSpec((count, pieces * cols), lambda i: (0, 0)),
        out_shape=jax.ShapeDtypeStruct((count, pieces * cols), BF16),
        scratch_shapes=[pltpu.VMEM((count, pieces * cols), F32)] * 2,
        name="gate_up",
    )(rows, *gates, *ups)


def down_kernel(*refs, groups):
    hiddens, downs, out_ref = refs[: len(groups)], refs[len(groups) : -1], refs[-1]
    total, at = None, 0
    for hidden, pieces in zip(hiddens, groups):
        cols = downs[at].shape[0]
        for i in range(pieces):
            term = dot(hidden[:, i * cols : (i + 1) * cols], downs[at][...])
            total = term if total is None else total + term
            at += 1
    out_ref[...] = total.astype(BF16)


def down(hiddens, groups):
    count = hiddens[0].shape[0]
    flat = [d for g in groups for d in g]
    inner, width = flat[0].shape
    part = width // 2
    return pl.pallas_call(
        functools.partial(down_kernel, groups=tuple(len(g) for g in groups)),
        grid=(2,),
        in_specs=[pl.BlockSpec(h.shape, lambda i: (0, 0)) for h in hiddens]
        + [pl.BlockSpec((inner, part), lambda i: (0, i))] * len(flat),
        out_specs=pl.BlockSpec((count, part), lambda i: (0, i)),
        out_shape=jax.ShapeDtypeStruct((count, width), BF16),
        name="down",
    )(*hiddens, *flat)


def combine_kernel(hi_ref, lo_ref, rows_ref, *refs):
    rows = rows_ref[...]
    first = ((0,), (0,))
    refs[-1][...] = (dot(hi_ref[...], rows, first) + dot(lo_ref[...], rows, first)).astype(BF16)


def combine(mix_hi, mix_lo, rows, at, width, before):
    slots, tokens = mix_hi.shape
    cols = rows.shape[1]
    part = cols // 2
    mix = pl.BlockSpec((slots, tokens), lambda i: (0, 0))
    in_specs = [mix, mix, pl.BlockSpec((slots, part), lambda i: (0, i))]
    operands = [mix_hi, mix_lo, rows]
    if before is not None:
        in_specs.append(pl.BlockSpec(memory_space=pl.ANY))
        operands.append(before)
    return pl.pallas_call(
        combine_kernel,
        grid=(2,),
        in_specs=in_specs,
        out_specs=pl.BlockSpec((tokens, part), lambda i: (0, i + 2 * at)),
        out_shape=jax.ShapeDtypeStruct((tokens, width), BF16),
        input_output_aliases={} if before is None else {3: 0},
        name="combine",
    )(*operands)


def swap(x, axis, bit):
    return lax.ppermute(x, axis, [(i, i ^ bit) for i in range(lax.axis_size(axis))])


def on_device(
    mixer_input,
    mixer_gain,
    query_weight,
    key_weight,
    value_weight,
    gate_weight,
    head_gain,
    output_weight,
    log_decay,
    expert_input,
    expert_gain,
    routes,
    route_weight,
    expert_gate,
    expert_up,
    expert_down,
):
    tp = lax.axis_size("tp")
    bits = []
    while (1 << len(bits)) < tp:
        bits.append(1 << len(bits))

    def spread(piece):
        pieces = [piece]
        for bit in reversed(bits):
            pieces = pieces + [swap(p, "tp", bit) for p in pieces]
        return pieces

    full = expert_down.shape[2]
    chunks = 2
    cut = full // chunks
    gates, ups = spread(expert_gate[0]), spread(expert_up[0])
    downs = [spread(expert_down[0][:, c * cut : (c + 1) * cut]) for c in range(chunks)]

    tokens, top = routes.shape
    experts = lax.axis_size("ep")
    capacity = max(2, 3 * tokens * top // (2 * experts))
    slots = experts * capacity
    width = expert_input.shape[1]
    outgoing, mix_hi, mix_lo = pl.pallas_call(
        functools.partial(dispatch_kernel, capacity=capacity),
        out_shape=(
            jax.ShapeDtypeStruct((slots, width), BF16),
            jax.ShapeDtypeStruct((slots, tokens), BF16),
            jax.ShapeDtypeStruct((slots, tokens), BF16),
        ),
        name="dispatch",
    )(expert_input, expert_gain.reshape(1, -1), routes.T, route_weight.T)
    arrived = lax.all_to_all(
        outgoing.reshape(experts, capacity, width), "ep", split_axis=0, concat_axis=0, tiled=True
    ).reshape(slots, width)

    rows = mixer_input.shape[0]
    heads = log_decay.shape[1]
    mix_width = query_weight.shape[1]
    head_dim = mix_width // heads
    half = head_dim // 2
    position = lax.axis_index("ep") * rows + jnp.arange(rows, dtype=jnp.int32)
    lane = jnp.arange(head_dim, dtype=jnp.int32)
    frequency = 10000.0 ** (-(lane % half).astype(F32) / half)
    angles = position.astype(F32)[:, None] * frequency[None, :]
    cosine = jnp.cos(angles)
    sine = jnp.where(lane < half, -1.0, 1.0)[None, :] * jnp.sin(angles)
    span = head_dim + PAD
    retained, queries, gate_raw, package = pl.pallas_call(
        functools.partial(retain_kernel, heads=heads, head_dim=head_dim),
        out_shape=(
            jax.ShapeDtypeStruct((rows, mix_width), F32),
            jax.ShapeDtypeStruct((rows, mix_width), BF16),
            jax.ShapeDtypeStruct((rows, mix_width), BF16),
            jax.ShapeDtypeStruct((experts, heads * span, head_dim), BF16),
        ),
        scratch_shapes=[pltpu.VMEM(mixer_input.shape, BF16)],
        name="retain",
    )(
        mixer_input,
        mixer_gain.reshape(1, -1),
        query_weight,
        key_weight,
        value_weight,
        gate_weight,
        cosine,
        sine,
        log_decay.T,
    )
    arrived, package = lax.optimization_barrier((arrived, package))
    packages = lax.all_to_all(package, "ep", split_axis=0, concat_axis=0, tiled=True)
    out_width = output_weight.shape[1]
    order = lax.axis_index("tp") ^ jnp.arange(tp + 1, dtype=jnp.int32)
    order = jnp.where(jnp.arange(tp + 1) < tp, order, lax.axis_index("ep")).astype(jnp.int32)
    vmem = pl.BlockSpec(memory_space=pltpu.VMEM)
    parts = pl.pallas_call(
        functools.partial(finish_kernel, heads=heads, head_dim=head_dim),
        in_specs=[pl.BlockSpec(memory_space=pltpu.SMEM)] + [vmem] * 6,
        out_specs=[vmem] * tp,
        out_shape=[jax.ShapeDtypeStruct((rows // tp, out_width), BF16)] * tp,
        scratch_shapes=[pltpu.VMEM((rows, mix_width), BF16)],
        name="finish",
    )(order, retained, queries, gate_raw, head_gain.reshape(1, -1), output_weight, packages)
    sums = [part for part in parts]
    for bit in bits:
        kept = range(0, len(sums), 2 * bit)
        for j in kept:
            other = swap(sums[j + bit].astype(BF16), "tp", bit)
            sums[j] = sums[j].astype(F32) + other.astype(F32)
    mixer_output = sums[0].astype(BF16)

    near, far = slice(0, None, 2), slice(1, None, 2)
    if tp > 2:
        split = [near, far]
    else:
        split = [slice(0, None)]
    hiddens = [gate_up(arrived, gates[s], ups[s]) for s in split]
    hiddens = list(lax.optimization_barrier((tuple(hiddens), parts[-1]))[0])
    expert_output = None
    for c in range(chunks):
        results = down(hiddens, [downs[c][s] for s in split])
        returned = lax.all_to_all(
            results.reshape(experts, capacity, cut), "ep", split_axis=0, concat_axis=0, tiled=True
        ).reshape(slots, cut)
        expert_output = combine(mix_hi, mix_lo, returned, c, full, expert_output)
    return (mixer_output, expert_output)


def solution(mesh):
    return jax.shard_map(
        on_device,
        mesh=mesh,
        in_specs=(
            P("ep", None),
            P(),
            P(None, "tp"),
            P(None, "tp"),
            P(None, "tp"),
            P(None, "tp"),
            P("tp"),
            P("tp", None),
            P("ep", "tp"),
            P(("ep", "tp"), None),
            P(),
            P(("ep", "tp"), None),
            P(("ep", "tp"), None),
            P("ep", None, "tp"),
            P("ep", None, "tp"),
            P("ep", "tp", None),
        ),
        out_specs=(P(("ep", "tp"), None), P(("ep", "tp"), None)),
        check_vma=False,
    )
```

profile of v0, /device:TPU:0, one launch (start us, length us, event | category | flops | bytes accessed | tf_op | source)
XLA Modules:
  0.0 154.2 jit_solution(4318338545498350171)
XLA Ops:
  0.6 3.0 %dispatch.1 = (bf16[384,2048]{1,0:T(8,128)(2,1)}, bf16[384,128]{1,0:T(8,128)(2,1)}, bf16[384,128]{1,0:T(8,128)(2,1)}) custom-call(bf16[128,2048]{1,0:T(8,128)(2,1)} %x_ref.3, f32[1,2048]{1,0:T(1,128)} %bitcast.29, s32[2,128]{1,0:T(2,128)} %bitcast.32, f32[2,128]{1,0:T(2,128)} %bitcast.33), custom_call_target="tpu_custom_call" | custom-call | tf_op jit(solution)/shard_map/dispatch/pallas_call | solution.py:306
  3.7 7.3 %all-to-all-start = ((bf16[8,48,2048]{2,1,0:T(8,128)(2,1)}), bf16[8,48,2048]{2,1,0:T(8,128)(2,1)S(1)}, u32[]{:S(2)}, u32[]{:S(2)}) async-start(bf16[8,48,2048]{2,1,0:T(8,128)(2,1)} %bitcast.21), calls=%async_computation | async-start | bytes 3145728 | tf_op jit(solution)/shard_map/all_to_all | solution.py:315
  14.8 1.6 %collective-permute-start.13 = (bf16[256,1024]{1,0:T(8,128)(2,1)S(1)}, bf16[256,1024]{1,0:T(8,128)(2,1)}, u32[]{:S(2)}, u32[]{:S(2)}) collective-permute-start(bf16[256,1024]{1,0:T(8,128)(2,1)S(1)} %get-tuple-element.32.refs_2_), channel_id=1, source_target_pairs={{0,2},{1,3},{2,0},{3,1},{4,6},{5,7},{6,4},{7,5},{8,10},{9,11},{10,... | collective-permute-start | bytes 1572872 | tf_op jit(solution)/shard_map/ppermute | solution.py:263
  16.4 20.9 %collective-permute-done.5.refs_0_ = bf16[2048,256]{1,0:T(8,128)(2,1)} collective-permute-done((bf16[2048,256]{1,0:T(8,128)(2,1)}, bf16[2048,256]{1,0:T(8,128)(2,1)}, u32[]{:S(2)}, u32[]{:S(2)}) %collective-permute-start.5) | collective-permute-done | bytes 1048608 | tf_op jit(solution)/shard_map/ppermute | solution.py:263
  37.3 22.5 %collective-permute-done.7.refs_2_ = bf16[2048,256]{1,0:T(8,128)(2,1)} collective-permute-done((bf16[2048,256]{1,0:T(8,128)(2,1)}, bf16[2048,256]{1,0:T(8,128)(2,1)}, u32[]{:S(2)}, u32[]{:S(2)}) %collective-permute-start.7) | collective-permute-done | bytes 1048608 | tf_op jit(solution)/shard_map/ppermute | solution.py:263
  59.8 1.8 %fusion = (f32[512,128]{1,0:T(8,128)}, f32[512,128]{1,0:T(8,128)}) fusion(f32[128]{0:T(128)S(1)} %get-tuple-element.36, f32[128]{0:T(128)S(1)} %get-tuple-element.37, f32[512]{0:T(512)S(1)} %add_convert_fusion.2), kind=kLoop, calls=%fused_computation.4 | loop fusion | flops 131072 | bytes 527360 | tf_op jit(solution)/shard_map/mul | solution.py:329
  61.6 8.9 %retain.1 = (f32[512,256]{1,0:T(8,128)}, bf16[512,256]{1,0:T(8,128)(2,1)}, bf16[512,256]{1,0:T(8,128)(2,1)}, bf16[8,288,128]{2,1,0:T(8,128)(2,1)}) custom-call(bf16[512,2048]{1,0:T(8,128)(2,1)} %x_ref.2, f32[1,2048]{1,0:T(1,128)} %bitcast.30, bf16[2048,256]{1,0:T(8,128)(2,1)} %wq_ref.1, bf16[2048,256]{1,0:T(8,128)(2,1)} %wk_ref.1, bf16[2048,256]{1,0:T(8,128)(2,1)} %wv_ref.1, ...), custom_call_target="tpu_custom_call" | custom-call | tf_op jit(solution)/shard_map/retain/pallas_call | solution.py:331
  70.5 6.0 %all-to-all-start.1 = ((bf16[8,288,128]{2,1,0:T(8,128)(2,1)}), bf16[8,288,128]{2,1,0:T(8,128)(2,1)S(1)}, u32[]{:S(2)}, u32[]{:S(2)}) async-start(bf16[8,288,128]{2,1,0:T(8,128)(2,1)} %get-tuple-element.22), calls=%async_computation.1 | async-start | bytes 1179648 | tf_op jit(solution)/shard_map/all_to_all | solution.py:353
  77.7 5.6 %gate_up.2.refs_0_ = bf16[384,512]{1,0:T(8,128)(2,1)} custom-call(bf16[384,2048]{1,0:T(8,128)(2,1)} %bitcast.15, bf16[2048,256]{1,0:T(8,128)(2,1)} %bitcast.25, bf16[2048,256]{1,0:T(8,128)(2,1)} %collective-permute-done.3.refs_1_, bf16[2048,256]{1,0:T(8,128)(2,1)} %bitcast.28, bf16[2048,256]{1,0:T(8,128)(2,1)} %collective-permute-done.4.refs_3_), custom_call_target="tpu_custom_call" | custom-call | tf_op jit(solution)/shard_map/gate_up/pallas_call | solution.py:196
  83.3 5.6 %gate_up.3.refs_1_ = bf16[384,512]{1,0:T(8,128)(2,1)} custom-call(bf16[384,2048]{1,0:T(8,128)(2,1)} %bitcast.16, bf16[2048,256]{1,0:T(8,128)(2,1)} %collective-permute-done.5.refs_0_, bf16[2048,256]{1,0:T(8,128)(2,1)} %collective-permute-done.6.refs_1_, bf16[2048,256]{1,0:T(8,128)(2,1)} %collective-permute-done.7.refs_2_, ...), custom_call_target="tpu_custom_call" | custom-call | tf_op jit(solution)/shard_map/gate_up/pallas_call | solution.py:196
  88.9 4.2 %all-to-all-done.1.pkg_ref = bf16[8,288,128]{2,1,0:T(8,128)(2,1)S(1)} async-done(((bf16[8,288,128]{2,1,0:T(8,128)(2,1)}), bf16[8,288,128]{2,1,0:T(8,128)(2,1)S(1)}, u32[]{:S(2)}, u32[]{:S(2)}) %all-to-all-start.1) | async-done | bytes 589856 | tf_op jit(solution)/shard_map/all_to_all | solution.py:353
  93.9 4.2 %finish.1 = (bf16[128,2048]{1,0:T(8,128)(2,1)}, bf16[128,2048]{1,0:T(8,128)(2,1)}, bf16[128,2048]{1,0:T(8,128)(2,1)}, bf16[128,2048]{1,0:T(8,128)(2,1)}) custom-call(s32[5]{0:T(128)} %compare_select_fusion.1.index_ref, f32[512,256]{1,0:T(8,128)} %get-tuple-element.17.ret_ref, bf16[512,256]{1,0:T(8,128)(2,1)} %get-tuple-element.18.qd_ref, ...), custom_call_target="tpu_custom_call" | custom-call | tf_op jit(solution)/shard_map/finish/pallas_call | solution.py:358
  98.1 3.5 %down.3 = bf16[384,1024]{1,0:T(8,128)(2,1)} custom-call(bf16[384,512]{1,0:T(8,128)(2,1)} %gate_up.2.refs_0_, bf16[384,512]{1,0:T(8,128)(2,1)} %gate_up.3.refs_1_, bf16[256,1024]{1,0:T(8,128)(2,1)} %copy-done.5, bf16[256,1024]{1,0:T(8,128)(2,1)} %collective-permute-done.12.refs_3_, bf16[256,1024]{1,0:T(8,128)(2,1)} %collective-permute-done.13.refs_4_, ...), custom_call_target="tpu_custom_call" | custom-call | tf_op jit(solution)/shard_map/down/pallas_call | solution.py:224
  101.6 3.8 %all-to-all-start.3 = ((bf16[8,48,1024]{2,1,0:T(8,128)(2,1)}), bf16[8,48,1024]{2,1,0:T(8,128)(2,1)S(1)}, u32[]{:S(2)}, u32[]{:S(2)}) async-start(bf16[8,48,1024]{2,1,0:T(8,128)(2,1)} %bitcast.17), calls=%async_computation.3 | async-start | bytes 1572864 | tf_op jit(solution)/shard_map/all_to_all | solution.py:384
  106.9 12.1 %collective-permute-done.10.refs_4_ = bf16[256,1024]{1,0:T(8,128)(2,1)S(1)} collective-permute-done((bf16[256,1024]{1,0:T(8,128)(2,1)S(1)}, bf16[256,1024]{1,0:T(8,128)(2,1)S(1)}, u32[]{:S(2)}, u32[]{:S(2)}) %collective-permute-start.10) | collective-permute-done | bytes 524320 | tf_op jit(solution)/shard_map/ppermute | solution.py:263
  119.5 1.5 collective-permute-done.11.refs_5_
  121.0 3.5 %down.2 = bf16[384,1024]{1,0:T(8,128)(2,1)} custom-call(bf16[384,512]{1,0:T(8,128)(2,1)} %gate_up.2.refs_0_, bf16[384,512]{1,0:T(8,128)(2,1)} %gate_up.3.refs_1_, bf16[256,1024]{1,0:T(8,128)(2,1)} %copy-done.4, bf16[256,1024]{1,0:T(8,128)(2,1)} %copy-done.8, bf16[256,1024]{1,0:T(8,128)(2,1)} %copy-done.7, bf16[256,1024]{1,0:T(8,128)(2,1)} %collective-permute-done.11.refs_5_), custom_call_target="tpu_custom_call" | custom-call | tf_op jit(solution)/shard_map/down/pallas_call | solution.py:224
  125.8 4.6 %all-to-all-start.2 = ((bf16[8,48,1024]{2,1,0:T(8,128)(2,1)}), bf16[8,48,1024]{2,1,0:T(8,128)(2,1)S(1)}, u32[]{:S(2)}, u32[]{:S(2)}) async-start(bf16[8,48,1024]{2,1,0:T(8,128)(2,1)} %bitcast.18), calls=%async_computation.2 | async-start | bytes 1572864 | tf_op jit(solution)/shard_map/all_to_all | solution.py:384
  130.6 1.6 %collective-permute-start.2 = (bf16[128,2048]{1,0:T(8,128)(2,1)S(1)}, bf16[128,2048]{1,0:T(8,128)(2,1)S(1)}, u32[]{:S(2)}, u32[]{:S(2)}) collective-permute-start(bf16[128,2048]{1,0:T(8,128)(2,1)S(1)} %add_convert_fusion.1), channel_id=1, source_target_pairs={{0,2},{1,3},{2,0},{3,1},{4,6},{5,7},{6,4},{7,5},{8,10},{9,11},{10,... | collective-permute-start | bytes 1572872 | tf_op jit(solution)/shard_map/ppermute | solution.py:263
  132.2 12.2 %collective-permute-done.2 = bf16[128,2048]{1,0:T(8,128)(2,1)S(1)} collective-permute-done((bf16[128,2048]{1,0:T(8,128)(2,1)S(1)}, bf16[128,2048]{1,0:T(8,128)(2,1)S(1)}, u32[]{:S(2)}, u32[]{:S(2)}) %collective-permute-start.2) | collective-permute-done | bytes 524320 | tf_op jit(solution)/shard_map/ppermute | solution.py:263
  144.3 2.1 %add_convert_fusion = bf16[128,2048]{1,0:T(8,128)(2,1)} fusion(bf16[128,2048]{1,0:T(8,128)(2,1)S(1)} %collective-permute-done.2, bf16[128,2048]{1,0:T(8,128)(2,1)} %collective-permute-done, bf16[128,2048]{1,0:T(8,128)(2,1)S(1)} %copy-done.9), kind=kLoop, calls=%fused_computation | loop fusion | flops 1572864 | bytes 2097152 | tf_op jit(solution)/shard_map/convert_element_type | solution.py:372
  146.4 2.4 %combine.2.refs_0_ = bf16[128,2048]{1,0:T(8,128)(2,1)} custom-call(bf16[384,128]{1,0:T(8,128)(2,1)} %get-tuple-element.27.hi_ref, bf16[384,128]{1,0:T(8,128)(2,1)} %get-tuple-element.28.lo_ref, bf16[384,1024]{1,0:T(8,128)(2,1)} %bitcast.19), custom_call_target="tpu_custom_call" | custom-call | tf_op jit(solution)/shard_map/combine/pallas_call | solution.py:251
  148.8 2.1 %all-to-all-done.2 = bf16[8,48,1024]{2,1,0:T(8,128)(2,1)S(1)} async-done(((bf16[8,48,1024]{2,1,0:T(8,128)(2,1)}), bf16[8,48,1024]{2,1,0:T(8,128)(2,1)S(1)}, u32[]{:S(2)}, u32[]{:S(2)}) %all-to-all-start.2) | async-done | bytes 786464 | tf_op jit(solution)/shard_map/all_to_all | solution.py:384
  151.8 2.4 %combine.3 = bf16[128,2048]{1,0:T(8,128)(2,1)} custom-call(bf16[384,128]{1,0:T(8,128)(2,1)} %get-tuple-element.27.hi_ref, bf16[384,128]{1,0:T(8,128)(2,1)} %get-tuple-element.28.lo_ref, bf16[384,1024]{1,0:T(8,128)(2,1)} %bitcast.20, bf16[128,2048]{1,0:T(8,128)(2,1)} %combine.2.refs_0_), custom_call_target="tpu_custom_call", output_to_operand_aliasing={{}: (3, {})} | custom-call | tf_op jit(solution)/shard_map/combine/pallas_call | solution.py:251
  (50 shorter events, 10.1 us)
Async XLA Ops:
  3.7 66.8 %all-to-all-start = ((bf16[8,48,2048]{2,1,0:T(8,128)(2,1)}), bf16[8,48,2048]{2,1,0:T(8,128)(2,1)S(1)}, u32[]{:S(2)}, u32[]{:S(2)}) async-start(bf16[8,48,2048]{2,1,0:T(8,128)(2,1)} %bitcast.21), calls=%async_computation | async-start | bytes 3145728 | tf_op jit(solution)/shard_map/all_to_all | solution.py:315
  10.9 26.3 %collective-permute-start.5 = (bf16[2048,256]{1,0:T(8,128)(2,1)}, bf16[2048,256]{1,0:T(8,128)(2,1)}, u32[]{:S(2)}, u32[]{:S(2)}) collective-permute-start(bf16[2048,256]{1,0:T(8,128)(2,1)} %bitcast.23), channel_id=1, source_target_pairs={{0,2},{1,3},{2,0},{3,1},{4,6},{5,7},{6,4},{7,5},{8,10},{9,11},{10,... | collective-permute-start | bytes 3145736 | tf_op jit(solution)/shard_map/ppermute | solution.py:263
  12.5 47.3 %collective-permute-start.7 = (bf16[2048,256]{1,0:T(8,128)(2,1)}, bf16[2048,256]{1,0:T(8,128)(2,1)}, u32[]{:S(2)}, u32[]{:S(2)}) collective-permute-start(bf16[2048,256]{1,0:T(8,128)(2,1)} %bitcast.26), channel_id=1, source_target_pairs={{0,2},{1,3},{2,0},{3,1},{4,6},{5,7},{6,4},{7,5},{8,10},{9,11},{10,... | collective-permute-start | bytes 3145736 | tf_op jit(solution)/shard_map/ppermute | solution.py:263
  13.0 63.9 %collective-permute-start.3 = (bf16[2048,256]{1,0:T(8,128)(2,1)}, bf16[2048,256]{1,0:T(8,128)(2,1)}, u32[]{:S(2)}, u32[]{:S(2)}) collective-permute-start(bf16[2048,256]{1,0:T(8,128)(2,1)} %bitcast.24), channel_id=1, source_target_pairs={{0,1},{1,0},{2,3},{3,2},{4,5},{5,4},{6,7},{7,6},{8,9},{9,8},{10,11... | collective-permute-start | bytes 3145736 | tf_op jit(solution)/shard_map/ppermute | solution.py:263
  13.0 64.7 %collective-permute-start.4 = (bf16[2048,256]{1,0:T(8,128)(2,1)}, bf16[2048,256]{1,0:T(8,128)(2,1)}, u32[]{:S(2)}, u32[]{:S(2)}) collective-permute-start(bf16[2048,256]{1,0:T(8,128)(2,1)} %bitcast.27), channel_id=1, source_target_pairs={{0,1},{1,0},{2,3},{3,2},{4,5},{5,4},{6,7},{7,6},{8,9},{9,8},{10,11... | collective-permute-start | bytes 3145736 | tf_op jit(solution)/shard_map/ppermute | solution.py:263
  14.7 61.8 %copy-start.5 = (bf16[256,1024]{1,0:T(8,128)(2,1)}, bf16[256,1024]{1,0:T(8,128)(2,1)S(1)}, u32[]{:S(2)}) copy-start(bf16[256,1024]{1,0:T(8,128)(2,1)S(1)} %get-tuple-element.32.refs_2_) | copy-start | bytes 1572868
  14.8 92.1 %copy-start.4 = (bf16[256,1024]{1,0:T(8,128)(2,1)}, bf16[256,1024]{1,0:T(8,128)(2,1)S(1)}, u32[]{:S(2)}) copy-start(bf16[256,1024]{1,0:T(8,128)(2,1)S(1)} %get-tuple-element.33.refs_2_) | copy-start | bytes 1572868
  14.8 61.8 %collective-permute-start.13 = (bf16[256,1024]{1,0:T(8,128)(2,1)S(1)}, bf16[256,1024]{1,0:T(8,128)(2,1)}, u32[]{:S(2)}, u32[]{:S(2)}) collective-permute-start(bf16[256,1024]{1,0:T(8,128)(2,1)S(1)} %get-tuple-element.32.refs_2_), channel_id=1, source_target_pairs={{0,2},{1,3},{2,0},{3,1},{4,6},{5,7},{6,4},{7,5},{8,10},{9,11},{10,... | collective-permute-start | bytes 1572872 | tf_op jit(solution)/shard_map/ppermute | solution.py:263
  37.3 46.0 %collective-permute-start.6 = (bf16[2048,256]{1,0:T(8,128)(2,1)}, bf16[2048,256]{1,0:T(8,128)(2,1)}, u32[]{:S(2)}, u32[]{:S(2)}) collective-permute-start(bf16[2048,256]{1,0:T(8,128)(2,1)} %collective-permute-done.5.refs_0_), channel_id=1, source_target_pairs={{0,1},{1,0},{2,3},{3,2},{4,5},{5,4},{6,7},{7,6},{8,9},{9,8},{10,11... | collective-permute-start | bytes 3145736 | tf_op jit(solution)/shard_map/ppermute | solution.py:263
  59.8 23.5 %collective-permute-start.8 = (bf16[2048,256]{1,0:T(8,128)(2,1)}, bf16[2048,256]{1,0:T(8,128)(2,1)}, u32[]{:S(2)}, u32[]{:S(2)}) collective-permute-start(bf16[2048,256]{1,0:T(8,128)(2,1)} %collective-permute-done.7.refs_2_), channel_id=1, source_target_pairs={{0,1},{1,0},{2,3},{3,2},{4,5},{5,4},{6,7},{7,6},{8,9},{9,8},{10,11... | collective-permute-start | bytes 3145736 | tf_op jit(solution)/shard_map/ppermute | solution.py:263
  70.5 7.2 %copy-start = (bf16[8,48,2048]{2,1,0:T(8,128)(2,1)}, bf16[8,48,2048]{2,1,0:T(8,128)(2,1)S(1)}, u32[]{:S(2)}) copy-start(bf16[8,48,2048]{2,1,0:T(8,128)(2,1)S(1)} %all-to-all-done) | copy-start | bytes 4718596
  70.5 22.6 %all-to-all-start.1 = ((bf16[8,288,128]{2,1,0:T(8,128)(2,1)}), bf16[8,288,128]{2,1,0:T(8,128)(2,1)S(1)}, u32[]{:S(2)}, u32[]{:S(2)}) async-start(bf16[8,288,128]{2,1,0:T(8,128)(2,1)} %get-tuple-element.22), calls=%async_computation.1 | async-start | bytes 1179648 | tf_op jit(solution)/shard_map/all_to_all | solution.py:353
  76.5 21.5 %collective-permute-start.12 = (bf16[256,1024]{1,0:T(8,128)(2,1)S(1)}, bf16[256,1024]{1,0:T(8,128)(2,1)}, u32[]{:S(2)}, u32[]{:S(2)}) collective-permute-start(bf16[256,1024]{1,0:T(8,128)(2,1)S(1)} %get-tuple-element.32.refs_2_), channel_id=1, source_target_pairs={{0,1},{1,0},{2,3},{3,2},{4,5},{5,4},{6,7},{7,6},{8,9},{9,8},{10,11... | collective-permute-start | bytes 1572872 | tf_op jit(solution)/shard_map/ppermute | solution.py:263
  76.8 21.3 %collective-permute-start.14 = (bf16[256,1024]{1,0:T(8,128)(2,1)}, bf16[256,1024]{1,0:T(8,128)(2,1)}, u32[]{:S(2)}, u32[]{:S(2)}) collective-permute-start(bf16[256,1024]{1,0:T(8,128)(2,1)} %collective-permute-done.13.refs_4_), channel_id=1, source_target_pairs={{0,1},{1,0},{2,3},{3,2},{4,5},{5,4},{6,7},{7,6},{8,9},{9,8},{10,11... | collective-permute-start | bytes 1572872 | tf_op jit(solution)/shard_map/ppermute | solution.py:263
  101.6 24.2 %all-to-all-start.3 = ((bf16[8,48,1024]{2,1,0:T(8,128)(2,1)}), bf16[8,48,1024]{2,1,0:T(8,128)(2,1)S(1)}, u32[]{:S(2)}, u32[]{:S(2)}) async-start(bf16[8,48,1024]{2,1,0:T(8,128)(2,1)} %bitcast.17), calls=%async_computation.3 | async-start | bytes 1572864 | tf_op jit(solution)/shard_map/all_to_all | solution.py:384
  105.4 13.6 %collective-permute-start.10 = (bf16[256,1024]{1,0:T(8,128)(2,1)S(1)}, bf16[256,1024]{1,0:T(8,128)(2,1)S(1)}, u32[]{:S(2)}, u32[]{:S(2)}) collective-permute-start(bf16[256,1024]{1,0:T(8,128)(2,1)S(1)} %get-tuple-element.33.refs_2_), channel_id=1, source_target_pairs={{0,2},{1,3},{2,0},{3,1},{4,6},{5,7},{6,4},{7,5},{8,10},{9,11},{10,... | collective-permute-start | bytes 1572872 | tf_op jit(solution)/shard_map/ppermute | solution.py:263
  106.9 12.6 %collective-permute-start.9 = (bf16[256,1024]{1,0:T(8,128)(2,1)S(1)}, bf16[256,1024]{1,0:T(8,128)(2,1)S(1)}, u32[]{:S(2)}, u32[]{:S(2)}) collective-permute-start(bf16[256,1024]{1,0:T(8,128)(2,1)S(1)} %get-tuple-element.33.refs_2_), channel_id=1, source_target_pairs={{0,1},{1,0},{2,3},{3,2},{4,5},{5,4},{6,7},{7,6},{8,9},{9,8},{10,11... | collective-permute-start | bytes 1572872 | tf_op jit(solution)/shard_map/ppermute | solution.py:263
  119.0 2.0 %collective-permute-start.11 = (bf16[256,1024]{1,0:T(8,128)(2,1)S(1)}, bf16[256,1024]{1,0:T(8,128)(2,1)}, u32[]{:S(2)}, u32[]{:S(2)}) collective-permute-start(bf16[256,1024]{1,0:T(8,128)(2,1)S(1)} %collective-permute-done.10.refs_4_), channel_id=1, source_target_pairs={{0,1},{1,0},{2,3},{3,2},{4,5},{5,4},{6,7},{7,6},{8,9},{9,8},{10,11... | collective-permute-start | bytes 1572872 | tf_op jit(solution)/shard_map/ppermute | solution.py:263
  119.0 11.5 %collective-permute-start.1 = (bf16[128,2048]{1,0:T(8,128)(2,1)}, bf16[128,2048]{1,0:T(8,128)(2,1)S(1)}, u32[]{:S(2)}, u32[]{:S(2)}) collective-permute-start(bf16[128,2048]{1,0:T(8,128)(2,1)} %get-tuple-element.26), channel_id=1, source_target_pairs={{0,1},{1,0},{2,3},{3,2},{4,5},{5,4},{6,7},{7,6},{8,9},{9,8},{10,11... | collective-permute-start | bytes 1572872 | tf_op jit(solution)/shard_map/ppermute | solution.py:263
  119.5 12.7 %collective-permute-start = (bf16[128,2048]{1,0:T(8,128)(2,1)}, bf16[128,2048]{1,0:T(8,128)(2,1)}, u32[]{:S(2)}, u32[]{:S(2)}) collective-permute-start(bf16[128,2048]{1,0:T(8,128)(2,1)} %get-tuple-element.24), channel_id=1, source_target_pairs={{0,1},{1,0},{2,3},{3,2},{4,5},{5,4},{6,7},{7,6},{8,9},{9,8},{10,11... | collective-permute-start | bytes 1572872 | tf_op jit(solution)/shard_map/ppermute | solution.py:263
  124.5 5.9 %copy-start.6 = (bf16[128,2048]{1,0:T(8,128)(2,1)S(1)}, bf16[128,2048]{1,0:T(8,128)(2,1)}, u32[]{:S(2)}) copy-start(bf16[128,2048]{1,0:T(8,128)(2,1)} %get-tuple-element.25) | copy-start | bytes 1572868
  125.8 18.6 %copy-start.9 = (bf16[128,2048]{1,0:T(8,128)(2,1)S(1)}, bf16[128,2048]{1,0:T(8,128)(2,1)}, u32[]{:S(2)}) copy-start(bf16[128,2048]{1,0:T(8,128)(2,1)} %get-tuple-element.23) | copy-start | bytes 1572868
  125.8 25.1 %all-to-all-start.2 = ((bf16[8,48,1024]{2,1,0:T(8,128)(2,1)}), bf16[8,48,1024]{2,1,0:T(8,128)(2,1)S(1)}, u32[]{:S(2)}, u32[]{:S(2)}) async-start(bf16[8,48,1024]{2,1,0:T(8,128)(2,1)} %bitcast.18), calls=%async_computation.2 | async-start | bytes 1572864 | tf_op jit(solution)/shard_map/all_to_all | solution.py:384
  130.6 13.7 %collective-permute-start.2 = (bf16[128,2048]{1,0:T(8,128)(2,1)S(1)}, bf16[128,2048]{1,0:T(8,128)(2,1)S(1)}, u32[]{:S(2)}, u32[]{:S(2)}) collective-permute-start(bf16[128,2048]{1,0:T(8,128)(2,1)S(1)} %add_convert_fusion.1), channel_id=1, source_target_pairs={{0,2},{1,3},{2,0},{3,1},{4,6},{5,7},{6,4},{7,5},{8,10},{9,11},{10,... | collective-permute-start | bytes 1572872 | tf_op jit(solution)/shard_map/ppermute | solution.py:263
  (5 other events, 10.1 us)
where the time goes:
time: 155 us; the launch traced here: 154 us
  waiting for transfers between devices  76.6 us (49%)
  Pallas kernels  39.2 us (25%)
  starting transfers between devices  30 us (19%)
  other arithmetic  4.56 us (3%)
  local copies, waits for them, and re-layouts  2.99 us (2%)
    ppermute x15, waiting for transfers between devices, swap(): lax.ppermute(x, axis, [(i, i ^ bit) for i in range(lax.axis_size(axis))])  69.2 us
    pallas_call x2, Pallas kernels, gate_up(): pl.pallas_call(functools.partial(gate_up_kernel, pieces=pieces), grid=(4,...  11.3 us
    pallas_call x1, Pallas kernels, on_device(): pl.pallas_call(functools.partial(retain_kernel, heads=heads, head_dim=hea...  8.92 us
    all_to_all x2, starting transfers between devices, on_device(): lax.all_to_all(results.reshape(experts, capacity, cut), 'ep', split_axis=...  8.44 us
    ppermute x15, starting transfers between devices, swap(): lax.ppermute(x, axis, [(i, i ^ bit) for i in range(lax.axis_size(axis))])  8.31 us
    all_to_all x1, starting transfers between devices, on_device(): lax.all_to_all(outgoing.reshape(experts, capacity, width), 'ep', split_ax...  7.28 us
    pallas_call x2, Pallas kernels, down(): pl.pallas_call(functools.partial(down_kernel, groups=tuple((len(g) for g...  7 us
    all_to_all x1, starting transfers between devices, on_device(): lax.all_to_all(package, 'ep', split_axis=0, concat_axis=0, tiled=True)  6.01 us
  transfers between devices with their start and end apart: 19, of which 8 were waited for; matrix products, arithmetic and copies ran while one was open for 4% of the time, Pallas kernels for 20%

commit v1 on v0

--- a/solution.py
+++ b/solution.py
@@ -232,31 +232,9 @@
     )(*hiddens, *flat)
 
 
-def combine_kernel(hi_ref, lo_ref, rows_ref, *refs):
-    rows = rows_ref[...]
+def combine(mix_hi, mix_lo, rows):
     first = ((0,), (0,))
-    refs[-1][...] = (dot(hi_ref[...], rows, first) + dot(lo_ref[...], rows, first)).astype(BF16)
-
-
-def combine(mix_hi, mix_lo, rows, at, width, before):
-    slots, tokens = mix_hi.shape
-    cols = rows.shape[1]
-    part = cols // 2
-    mix = pl.BlockSpec((slots, tokens), lambda i: (0, 0))
-    in_specs = [mix, mix, pl.BlockSpec((slots, part), lambda i: (0, i))]
-    operands = [mix_hi, mix_lo, rows]
-    if before is not None:
-        in_specs.append(pl.BlockSpec(memory_space=pl.ANY))
-        operands.append(before)
-    return pl.pallas_call(
-        combine_kernel,
-        grid=(2,),
-        in_specs=in_specs,
-        out_specs=pl.BlockSpec((tokens, part), lambda i: (0, i + 2 * at)),
-        out_shape=jax.ShapeDtypeStruct((tokens, width), BF16),
-        input_output_aliases={} if before is None else {3: 0},
-        name="combine",
-    )(*operands)
+    return (dot(mix_hi, rows, first) + dot(mix_lo, rows, first)).astype(BF16)
 
 
 def swap(x, axis, bit):
@@ -351,6 +329,17 @@
     )
     arrived, package = lax.optimization_barrier((arrived, package))
     packages = lax.all_to_all(package, "ep", split_axis=0, concat_axis=0, tiled=True)
+    near, far = slice(0, None, 2), slice(1, None, 2)
+    if tp > 2:
+        split = [near, far]
+    else:
+        split = [slice(0, None)]
+    hiddens = []
+    for part in split:
+        hiddens.append(gate_up(arrived, gates[part], ups[part]))
+    first = down(hiddens, [downs[0][part] for part in split])
+    packages = lax.optimization_barrier((packages, first))[0]
+
     out_width = output_weight.shape[1]
     order = lax.axis_index("tp") ^ jnp.arange(tp + 1, dtype=jnp.int32)
     order = jnp.where(jnp.arange(tp + 1) < tp, order, lax.axis_index("ep")).astype(jnp.int32)
@@ -371,20 +360,15 @@
             sums[j] = sums[j].astype(F32) + other.astype(F32)
     mixer_output = sums[0].astype(BF16)
 
-    near, far = slice(0, None, 2), slice(1, None, 2)
-    if tp > 2:
-        split = [near, far]
-    else:
-        split = [slice(0, None)]
-    hiddens = [gate_up(arrived, gates[s], ups[s]) for s in split]
     hiddens = list(lax.optimization_barrier((tuple(hiddens), parts[-1]))[0])
-    expert_output = None
+    columns = []
     for c in range(chunks):
-        results = down(hiddens, [downs[c][s] for s in split])
+        results = down(hiddens, [downs[c][part] for part in split]) if c else first
         returned = lax.all_to_all(
             results.reshape(experts, capacity, cut), "ep", split_axis=0, concat_axis=0, tiled=True
         ).reshape(slots, cut)
-        expert_output = combine(mix_hi, mix_lo, returned, c, full, expert_output)
+        columns.append(combine(mix_hi, mix_lo, returned))
+    expert_output = jnp.concatenate(columns, axis=1)
     return (mixer_output, expert_output)
 
 

time: 155 us -> 150 us (0.968)
  Pallas kernels: 39.2 us -> 34.6 us
  waiting for transfers between devices: 76.6 us -> 73.3 us
  starting transfers between devices: 30 us -> 32.4 us
    pallas_call x2 -> x0, Pallas kernels: 4.79 us -> none  [combine(): pl.pallas_call(combine_kernel, grid=(2,), in_specs=in_specs, out_specs=pl...]
    all_to_all x1, waiting for transfers between devices: 4.15 us -> 1.18 us  [on_device(): lax.all_to_all(package, 'ep', split_axis=0, concat_axis=0, tiled=True)]
    ppermute x15, waiting for transfers between devices: 69.2 us -> 66.6 us  [swap(): lax.ppermute(x, axis, [(i, i ^ bit) for i in range(lax.axis_size(axis))])]
    all_to_all x2, starting transfers between devices: 8.44 us -> 10.8 us  [on_device(): lax.all_to_all(results.reshape(experts, capacity, cut), 'ep', split_axis=...]
    all_to_all x2, waiting for transfers between devices: 3.31 us -> 5.49 us  [on_device(): lax.all_to_all(results.reshape(experts, capacity, cut), 'ep', split_axis=...]
  transfers between devices with their start and end apart: 19 -> 19, of which waited for: 8 -> 6; matrix products, arithmetic and copies ran while one was open for 4% -> 4% of each run, Pallas kernels for 20% -> 21%
where the time goes in v1:
time: 150 us; the launch traced here: 149 us
  waiting for transfers between devices  73.3 us (49%)
  Pallas kernels  34.6 us (23%)
  starting transfers between devices  32.4 us (22%)
  other arithmetic  4.37 us (3%)
  local copies, waits for them, and re-layouts  2.09 us (1%)
    ppermute x15, waiting for transfers between devices, swap(): lax.ppermute(x, axis, [(i, i ^ bit) for i in range(lax.axis_size(axis))])  66.6 us
    pallas_call x2, Pallas kernels, gate_up(): pl.pallas_call(functools.partial(gate_up_kernel, pieces=pieces), grid=(4,...  11.3 us
    all_to_all x2, starting transfers between devices, on_device(): lax.all_to_all(results.reshape(experts, capacity, cut), 'ep', split_axis=...  10.8 us
    pallas_call x1, Pallas kernels, on_device(): pl.pallas_call(functools.partial(retain_kernel, heads=heads, head_dim=hea...  8.92 us
    ppermute x15, starting transfers between devices, swap(): lax.ppermute(x, axis, [(i, i ^ bit) for i in range(lax.axis_size(axis))])  8.31 us
    all_to_all x1, starting transfers between devices, on_device(): lax.all_to_all(outgoing.reshape(experts, capacity, width), 'ep', split_ax...  7.28 us
    pallas_call x2, Pallas kernels, down(): pl.pallas_call(functools.partial(down_kernel, groups=tuple((len(g) for g...  6.98 us
    all_to_all x1, starting transfers between devices, on_device(): lax.all_to_all(package, 'ep', split_axis=0, concat_axis=0, tiled=True)  6.01 us
  transfers between devices with their start and end apart: 19, of which 6 were waited for; matrix products, arithmetic and copies ran while one was open for 4% of the time, Pallas kernels for 21%

profile of v1, /device:TPU:0, one launch (start us, length us, event | category | flops | bytes accessed | tf_op | source)
XLA Modules:
  0.0 148.9 jit_solution(10317577021014570837)
XLA Ops:
  0.6 3.0 %dispatch.1 = (bf16[384,2048]{1,0:T(8,128)(2,1)}, bf16[384,128]{1,0:T(8,128)(2,1)}, bf16[384,128]{1,0:T(8,128)(2,1)}) custom-call(bf16[128,2048]{1,0:T(8,128)(2,1)} %x_ref.3, f32[1,2048]{1,0:T(1,128)} %bitcast.33, s32[2,128]{1,0:T(2,128)} %bitcast.36, f32[2,128]{1,0:T(2,128)} %bitcast.37), custom_call_target="tpu_custom_call" | custom-call | tf_op jit(solution)/shard_map/dispatch/pallas_call | solution.py:284
  3.7 7.3 %all-to-all-start = ((bf16[8,48,2048]{2,1,0:T(8,128)(2,1)}), bf16[8,48,2048]{2,1,0:T(8,128)(2,1)S(1)}, u32[]{:S(2)}, u32[]{:S(2)}) async-start(bf16[8,48,2048]{2,1,0:T(8,128)(2,1)} %bitcast.31), calls=%async_computation | async-start | bytes 3145728 | tf_op jit(solution)/shard_map/all_to_all | solution.py:293
  10.9 1.5 %collective-permute-start.2 = (bf16[2048,256]{1,0:T(8,128)(2,1)}, bf16[2048,256]{1,0:T(8,128)(2,1)}, u32[]{:S(2)}, u32[]{:S(2)}) collective-permute-start(bf16[2048,256]{1,0:T(8,128)(2,1)} %bitcast.8.refs_0_), channel_id=1, source_target_pairs={{0,2},{1,3},{2,0},{3,1},{4,6},{5,7},{6,4},{7,5},{8,10},{9,11},{10,... | collective-permute-start | bytes 3145736 | tf_op jit(solution)/shard_map/ppermute | solution.py:241
  13.5 23.8 %collective-permute-done.2.refs_0_ = bf16[2048,256]{1,0:T(8,128)(2,1)} collective-permute-done((bf16[2048,256]{1,0:T(8,128)(2,1)}, bf16[2048,256]{1,0:T(8,128)(2,1)}, u32[]{:S(2)}, u32[]{:S(2)}) %collective-permute-start.2) | collective-permute-done | bytes 1048608 | tf_op jit(solution)/shard_map/ppermute | solution.py:241
  37.3 1.3 fusion.7
  38.6 1.6 %collective-permute-start.7 = (bf16[256,1024]{1,0:T(8,128)(2,1)S(1)}, bf16[256,1024]{1,0:T(8,128)(2,1)}, u32[]{:S(2)}, u32[]{:S(2)}) collective-permute-start(bf16[256,1024]{1,0:T(8,128)(2,1)S(1)} %get-tuple-element.35.refs_2_), channel_id=1, source_target_pairs={{0,2},{1,3},{2,0},{3,1},{4,6},{5,7},{6,4},{7,5},{8,10},{9,11},{10,... | collective-permute-start | bytes 1572872 | tf_op jit(solution)/shard_map/ppermute | solution.py:241
  40.2 19.6 %collective-permute-done.4.refs_2_ = bf16[2048,256]{1,0:T(8,128)(2,1)} collective-permute-done((bf16[2048,256]{1,0:T(8,128)(2,1)}, bf16[2048,256]{1,0:T(8,128)(2,1)}, u32[]{:S(2)}, u32[]{:S(2)}) %collective-permute-start.4) | collective-permute-done | bytes 1048608 | tf_op jit(solution)/shard_map/ppermute | solution.py:241
  59.8 1.8 %fusion.2 = (f32[512,128]{1,0:T(8,128)}, f32[512,128]{1,0:T(8,128)}) fusion(f32[128]{0:T(128)S(1)} %get-tuple-element.38, f32[128]{0:T(128)S(1)} %get-tuple-element.39, f32[512]{0:T(512)S(1)} %add_convert_fusion.2), kind=kLoop, calls=%fused_computation.9 | loop fusion | flops 131072 | bytes 527360 | tf_op jit(solution)/shard_map/mul | solution.py:307
  61.6 8.9 %retain.1 = (f32[512,256]{1,0:T(8,128)}, bf16[512,256]{1,0:T(8,128)(2,1)}, bf16[512,256]{1,0:T(8,128)(2,1)}, bf16[8,288,128]{2,1,0:T(8,128)(2,1)}) custom-call(bf16[512,2048]{1,0:T(8,128)(2,1)} %x_ref.2, f32[1,2048]{1,0:T(1,128)} %bitcast.34, bf16[2048,256]{1,0:T(8,128)(2,1)} %wq_ref.1, bf16[2048,256]{1,0:T(8,128)(2,1)} %wk_ref.1, bf16[2048,256]{1,0:T(8,128)(2,1)} %wv_ref.1, ...), custom_call_target="tpu_custom_call" | custom-call | tf_op jit(solution)/shard_map/retain/pallas_call | solution.py:309
  70.5 6.0 %all-to-all-start.1 = ((bf16[8,288,128]{2,1,0:T(8,128)(2,1)}), bf16[8,288,128]{2,1,0:T(8,128)(2,1)S(1)}, u32[]{:S(2)}, u32[]{:S(2)}) async-start(bf16[8,288,128]{2,1,0:T(8,128)(2,1)} %get-tuple-element.23), calls=%async_computation.1 | async-start | bytes 1179648 | tf_op jit(solution)/shard_map/all_to_all | solution.py:331
  77.1 5.6 %gate_up.3.refs_1_ = bf16[384,512]{1,0:T(8,128)(2,1)} custom-call(bf16[384,2048]{1,0:T(8,128)(2,1)} %bitcast.23, bf16[2048,256]{1,0:T(8,128)(2,1)} %collective-permute-done.2.refs_0_, bf16[2048,256]{1,0:T(8,128)(2,1)} %collective-permute-done.3.refs_1_, bf16[2048,256]{1,0:T(8,128)(2,1)} %collective-permute-done.4.refs_2_, ...), custom_call_target="tpu_custom_call" | custom-call | tf_op jit(solution)/shard_map/gate_up/pallas_call | solution.py:196
  82.7 5.7 %gate_up.2.refs_0_ = bf16[384,512]{1,0:T(8,128)(2,1)} custom-call(bf16[384,2048]{1,0:T(8,128)(2,1)} %bitcast.24, bf16[2048,256]{1,0:T(8,128)(2,1)} %bitcast.8.refs_0_, bf16[2048,256]{1,0:T(8,128)(2,1)} %collective-permute-done.refs_1_, bf16[2048,256]{1,0:T(8,128)(2,1)} %bitcast.9.refs_2_, bf16[2048,256]{1,0:T(8,128)(2,1)} %collective-permute-done.1.refs_3_), custom_call_target="tpu_custom_call" | custom-call | tf_op jit(solution)/shard_map/gate_up/pallas_call | solution.py:196
  88.4 3.5 %down.2 = bf16[384,1024]{1,0:T(8,128)(2,1)} custom-call(bf16[384,512]{1,0:T(8,128)(2,1)} %gate_up.2.refs_0_, bf16[384,512]{1,0:T(8,128)(2,1)} %gate_up.3.refs_1_, bf16[256,1024]{1,0:T(8,128)(2,1)} %copy-done.3, bf16[256,1024]{1,0:T(8,128)(2,1)} %collective-permute-done.6.refs_3_, bf16[256,1024]{1,0:T(8,128)(2,1)} %collective-permute-done.7.refs_4_, ...), custom_call_target="tpu_custom_call" | custom-call | tf_op jit(solution)/shard_map/down/pallas_call | solution.py:224
  91.9 1.2 all-to-all-done.1.pkg_ref
  93.1 4.8 %all-to-all-start.2 = ((bf16[8,48,1024]{2,1,0:T(8,128)(2,1)}), bf16[8,48,1024]{2,1,0:T(8,128)(2,1)S(1)}, u32[]{:S(2)}, u32[]{:S(2)}) async-start(bf16[8,48,1024]{2,1,0:T(8,128)(2,1)} %bitcast.29), calls=%async_computation.2 | async-start | bytes 1572864 | tf_op jit(solution)/shard_map/all_to_all | solution.py:367
  97.9 1.5 %collective-permute-start.13 = (bf16[256,1024]{1,0:T(8,128)(2,1)S(1)}, bf16[256,1024]{1,0:T(8,128)(2,1)S(1)}, u32[]{:S(2)}, u32[]{:S(2)}) collective-permute-start(bf16[256,1024]{1,0:T(8,128)(2,1)S(1)} %get-tuple-element.34.refs_2_), channel_id=1, source_target_pairs={{0,2},{1,3},{2,0},{3,1},{4,6},{5,7},{6,4},{7,5},{8,10},{9,11},{10,... | collective-permute-start | bytes 1572872 | tf_op jit(solution)/shard_map/ppermute | solution.py:241
  100.0 11.5 %collective-permute-done.13.refs_4_ = bf16[256,1024]{1,0:T(8,128)(2,1)S(1)} collective-permute-done((bf16[256,1024]{1,0:T(8,128)(2,1)S(1)}, bf16[256,1024]{1,0:T(8,128)(2,1)S(1)}, u32[]{:S(2)}, u32[]{:S(2)}) %collective-permute-start.13) | collective-permute-done | bytes 524320 | tf_op jit(solution)/shard_map/ppermute | solution.py:241
  111.5 4.4 %finish.1 = (bf16[128,2048]{1,0:T(8,128)(2,1)}, bf16[128,2048]{1,0:T(8,128)(2,1)}, bf16[128,2048]{1,0:T(8,128)(2,1)}, bf16[128,2048]{1,0:T(8,128)(2,1)}) custom-call(s32[5]{0:T(128)} %compare_select_fusion.1.index_ref, f32[512,256]{1,0:T(8,128)} %get-tuple-element.18.ret_ref, bf16[512,256]{1,0:T(8,128)(2,1)} %get-tuple-element.19.qd_ref, ...), custom_call_target="tpu_custom_call" | custom-call | tf_op jit(solution)/shard_map/finish/pallas_call | solution.py:347
  117.2 3.5 %down.3 = bf16[384,1024]{1,0:T(8,128)(2,1)} custom-call(bf16[384,512]{1,0:T(8,128)(2,1)} %gate_up.2.refs_0_, bf16[384,512]{1,0:T(8,128)(2,1)} %gate_up.3.refs_1_, bf16[256,1024]{1,0:T(8,128)(2,1)} %copy-done.2, bf16[256,1024]{1,0:T(8,128)(2,1)} %copy-done.5, bf16[256,1024]{1,0:T(8,128)(2,1)} %copy-done.4, bf16[256,1024]{1,0:T(8,128)(2,1)} %collective-permute-done.14.refs_5_), custom_call_target="tpu_custom_call" | custom-call | tf_op jit(solution)/shard_map/down/pallas_call | solution.py:224
  120.7 6.0 %all-to-all-start.3 = ((bf16[8,48,1024]{2,1,0:T(8,128)(2,1)}), bf16[8,48,1024]{2,1,0:T(8,128)(2,1)S(1)}, u32[]{:S(2)}, u32[]{:S(2)}) async-start(bf16[8,48,1024]{2,1,0:T(8,128)(2,1)} %bitcast.30), calls=%async_computation.3 | async-start | bytes 1572864 | tf_op jit(solution)/shard_map/all_to_all | solution.py:367
  126.9 1.6 %collective-permute-start.11 = (bf16[128,2048]{1,0:T(8,128)(2,1)S(1)}, bf16[128,2048]{1,0:T(8,128)(2,1)S(1)}, u32[]{:S(2)}, u32[]{:S(2)}) collective-permute-start(bf16[128,2048]{1,0:T(8,128)(2,1)S(1)} %add_convert_fusion.1), channel_id=1, source_target_pairs={{0,2},{1,3},{2,0},{3,1},{4,6},{5,7},{6,4},{7,5},{8,10},{9,11},{10,... | collective-permute-start | bytes 1572872 | tf_op jit(solution)/shard_map/ppermute | solution.py:241
  129.2 11.7 %collective-permute-done.11 = bf16[128,2048]{1,0:T(8,128)(2,1)S(1)} collective-permute-done((bf16[128,2048]{1,0:T(8,128)(2,1)S(1)}, bf16[128,2048]{1,0:T(8,128)(2,1)S(1)}, u32[]{:S(2)}, u32[]{:S(2)}) %collective-permute-start.11) | collective-permute-done | bytes 524320 | tf_op jit(solution)/shard_map/ppermute | solution.py:241
  140.9 1.0 add_convert_fusion
  141.9 5.5 %all-to-all-done.3 = bf16[8,48,1024]{2,1,0:T(8,128)(2,1)S(1)} async-done(((bf16[8,48,1024]{2,1,0:T(8,128)(2,1)}), bf16[8,48,1024]{2,1,0:T(8,128)(2,1)S(1)}, u32[]{:S(2)}, u32[]{:S(2)}) %all-to-all-start.3) | async-done | bytes 786464 | tf_op jit(solution)/shard_map/all_to_all | solution.py:367
  (55 shorter events, 5.8 us)
Async XLA Ops:
  3.7 66.8 %all-to-all-start = ((bf16[8,48,2048]{2,1,0:T(8,128)(2,1)}), bf16[8,48,2048]{2,1,0:T(8,128)(2,1)S(1)}, u32[]{:S(2)}, u32[]{:S(2)}) async-start(bf16[8,48,2048]{2,1,0:T(8,128)(2,1)} %bitcast.31), calls=%async_computation | async-start | bytes 3145728 | tf_op jit(solution)/shard_map/all_to_all | solution.py:293
  10.9 26.3 %collective-permute-start.2 = (bf16[2048,256]{1,0:T(8,128)(2,1)}, bf16[2048,256]{1,0:T(8,128)(2,1)}, u32[]{:S(2)}, u32[]{:S(2)}) collective-permute-start(bf16[2048,256]{1,0:T(8,128)(2,1)} %bitcast.8.refs_0_), channel_id=1, source_target_pairs={{0,2},{1,3},{2,0},{3,1},{4,6},{5,7},{6,4},{7,5},{8,10},{9,11},{10,... | collective-permute-start | bytes 3145736 | tf_op jit(solution)/shard_map/ppermute | solution.py:241
  12.5 47.3 %collective-permute-start.4 = (bf16[2048,256]{1,0:T(8,128)(2,1)}, bf16[2048,256]{1,0:T(8,128)(2,1)}, u32[]{:S(2)}, u32[]{:S(2)}) collective-permute-start(bf16[2048,256]{1,0:T(8,128)(2,1)} %bitcast.9.refs_2_), channel_id=1, source_target_pairs={{0,2},{1,3},{2,0},{3,1},{4,6},{5,7},{6,4},{7,5},{8,10},{9,11},{10,... | collective-permute-start | bytes 3145736 | tf_op jit(solution)/shard_map/ppermute | solution.py:241
  13.0 69.8 %collective-permute-start = (bf16[2048,256]{1,0:T(8,128)(2,1)}, bf16[2048,256]{1,0:T(8,128)(2,1)}, u32[]{:S(2)}, u32[]{:S(2)}) collective-permute-start(bf16[2048,256]{1,0:T(8,128)(2,1)} %bitcast.8.refs_0_), channel_id=1, source_target_pairs={{0,1},{1,0},{2,3},{3,2},{4,5},{5,4},{6,7},{7,6},{8,9},{9,8},{10,11... | collective-permute-start | bytes 3145736 | tf_op jit(solution)/shard_map/ppermute | solution.py:241
  13.0 69.8 %collective-permute-start.1 = (bf16[2048,256]{1,0:T(8,128)(2,1)}, bf16[2048,256]{1,0:T(8,128)(2,1)}, u32[]{:S(2)}, u32[]{:S(2)}) collective-permute-start(bf16[2048,256]{1,0:T(8,128)(2,1)} %bitcast.9.refs_2_), channel_id=1, source_target_pairs={{0,1},{1,0},{2,3},{3,2},{4,5},{5,4},{6,7},{7,6},{8,9},{9,8},{10,11... | collective-permute-start | bytes 3145736 | tf_op jit(solution)/shard_map/ppermute | solution.py:241
  37.3 39.5 %collective-permute-start.3 = (bf16[2048,256]{1,0:T(8,128)(2,1)}, bf16[2048,256]{1,0:T(8,128)(2,1)}, u32[]{:S(2)}, u32[]{:S(2)}) collective-permute-start(bf16[2048,256]{1,0:T(8,128)(2,1)} %collective-permute-done.2.refs_0_), channel_id=1, source_target_pairs={{0,1},{1,0},{2,3},{3,2},{4,5},{5,4},{6,7},{7,6},{8,9},{9,8},{10,11... | collective-permute-start | bytes 3145736 | tf_op jit(solution)/shard_map/ppermute | solution.py:241
  38.6 38.0 %copy-start.3 = (bf16[256,1024]{1,0:T(8,128)(2,1)}, bf16[256,1024]{1,0:T(8,128)(2,1)S(1)}, u32[]{:S(2)}) copy-start(bf16[256,1024]{1,0:T(8,128)(2,1)S(1)} %get-tuple-element.35.refs_2_) | copy-start | bytes 1572868
  38.6 60.8 %copy-start.2 = (bf16[256,1024]{1,0:T(8,128)(2,1)}, bf16[256,1024]{1,0:T(8,128)(2,1)S(1)}, u32[]{:S(2)}) copy-start(bf16[256,1024]{1,0:T(8,128)(2,1)S(1)} %get-tuple-element.34.refs_2_) | copy-start | bytes 1572868
  38.6 37.9 %collective-permute-start.7 = (bf16[256,1024]{1,0:T(8,128)(2,1)S(1)}, bf16[256,1024]{1,0:T(8,128)(2,1)}, u32[]{:S(2)}, u32[]{:S(2)}) collective-permute-start(bf16[256,1024]{1,0:T(8,128)(2,1)S(1)} %get-tuple-element.35.refs_2_), channel_id=1, source_target_pairs={{0,2},{1,3},{2,0},{3,1},{4,6},{5,7},{6,4},{7,5},{8,10},{9,11},{10,... | collective-permute-start | bytes 1572872 | tf_op jit(solution)/shard_map/ppermute | solution.py:241
  59.8 17.4 %collective-permute-start.5 = (bf16[2048,256]{1,0:T(8,128)(2,1)}, bf16[2048,256]{1,0:T(8,128)(2,1)}, u32[]{:S(2)}, u32[]{:S(2)}) collective-permute-start(bf16[2048,256]{1,0:T(8,128)(2,1)} %collective-permute-done.4.refs_2_), channel_id=1, source_target_pairs={{0,1},{1,0},{2,3},{3,2},{4,5},{5,4},{6,7},{7,6},{8,9},{9,8},{10,11... | collective-permute-start | bytes 3145736 | tf_op jit(solution)/shard_map/ppermute | solution.py:241
  70.5 22.6 %all-to-all-start.1 = ((bf16[8,288,128]{2,1,0:T(8,128)(2,1)}), bf16[8,288,128]{2,1,0:T(8,128)(2,1)S(1)}, u32[]{:S(2)}, u32[]{:S(2)}) async-start(bf16[8,288,128]{2,1,0:T(8,128)(2,1)} %get-tuple-element.23), calls=%async_computation.1 | async-start | bytes 1179648 | tf_op jit(solution)/shard_map/all_to_all | solution.py:331
  76.5 11.9 %collective-permute-start.6 = (bf16[256,1024]{1,0:T(8,128)(2,1)S(1)}, bf16[256,1024]{1,0:T(8,128)(2,1)}, u32[]{:S(2)}, u32[]{:S(2)}) collective-permute-start(bf16[256,1024]{1,0:T(8,128)(2,1)S(1)} %get-tuple-element.35.refs_2_), channel_id=1, source_target_pairs={{0,1},{1,0},{2,3},{3,2},{4,5},{5,4},{6,7},{7,6},{8,9},{9,8},{10,11... | collective-permute-start | bytes 1572872 | tf_op jit(solution)/shard_map/ppermute | solution.py:241
  76.8 11.6 %collective-permute-start.8 = (bf16[256,1024]{1,0:T(8,128)(2,1)}, bf16[256,1024]{1,0:T(8,128)(2,1)}, u32[]{:S(2)}, u32[]{:S(2)}) collective-permute-start(bf16[256,1024]{1,0:T(8,128)(2,1)} %collective-permute-done.7.refs_4_), channel_id=1, source_target_pairs={{0,1},{1,0},{2,3},{3,2},{4,5},{5,4},{6,7},{7,6},{8,9},{9,8},{10,11... | collective-permute-start | bytes 1572872 | tf_op jit(solution)/shard_map/ppermute | solution.py:241
  93.1 18.5 %copy-start.1 = (bf16[8,288,128]{2,1,0:T(8,128)(2,1)}, bf16[8,288,128]{2,1,0:T(8,128)(2,1)S(1)}, u32[]{:S(2)}) copy-start(bf16[8,288,128]{2,1,0:T(8,128)(2,1)S(1)} %all-to-all-done.1.pkg_ref) | copy-start | bytes 1769476
  93.1 27.7 %all-to-all-start.2 = ((bf16[8,48,1024]{2,1,0:T(8,128)(2,1)}), bf16[8,48,1024]{2,1,0:T(8,128)(2,1)S(1)}, u32[]{:S(2)}, u32[]{:S(2)}) async-start(bf16[8,48,1024]{2,1,0:T(8,128)(2,1)} %bitcast.29), calls=%async_computation.2 | async-start | bytes 1572864 | tf_op jit(solution)/shard_map/all_to_all | solution.py:367
  97.9 13.6 %collective-permute-start.13 = (bf16[256,1024]{1,0:T(8,128)(2,1)S(1)}, bf16[256,1024]{1,0:T(8,128)(2,1)S(1)}, u32[]{:S(2)}, u32[]{:S(2)}) collective-permute-start(bf16[256,1024]{1,0:T(8,128)(2,1)S(1)} %get-tuple-element.34.refs_2_), channel_id=1, source_target_pairs={{0,2},{1,3},{2,0},{3,1},{4,6},{5,7},{6,4},{7,5},{8,10},{9,11},{10,... | collective-permute-start | bytes 1572872 | tf_op jit(solution)/shard_map/ppermute | solution.py:241
  99.4 17.0 %collective-permute-start.12 = (bf16[256,1024]{1,0:T(8,128)(2,1)S(1)}, bf16[256,1024]{1,0:T(8,128)(2,1)S(1)}, u32[]{:S(2)}, u32[]{:S(2)}) collective-permute-start(bf16[256,1024]{1,0:T(8,128)(2,1)S(1)} %get-tuple-element.34.refs_2_), channel_id=1, source_target_pairs={{0,1},{1,0},{2,3},{3,2},{4,5},{5,4},{6,7},{7,6},{8,9},{9,8},{10,11... | collective-permute-start | bytes 1572872 | tf_op jit(solution)/shard_map/ppermute | solution.py:241
  111.5 4.9 %collective-permute-start.14 = (bf16[256,1024]{1,0:T(8,128)(2,1)S(1)}, bf16[256,1024]{1,0:T(8,128)(2,1)}, u32[]{:S(2)}, u32[]{:S(2)}) collective-permute-start(bf16[256,1024]{1,0:T(8,128)(2,1)S(1)} %collective-permute-done.13.refs_4_), channel_id=1, source_target_pairs={{0,1},{1,0},{2,3},{3,2},{4,5},{5,4},{6,7},{7,6},{8,9},{9,8},{10,11... | collective-permute-start | bytes 1572872 | tf_op jit(solution)/shard_map/ppermute | solution.py:241
  115.9 10.9 %collective-permute-start.10 = (bf16[128,2048]{1,0:T(8,128)(2,1)}, bf16[128,2048]{1,0:T(8,128)(2,1)S(1)}, u32[]{:S(2)}, u32[]{:S(2)}) collective-permute-start(bf16[128,2048]{1,0:T(8,128)(2,1)} %get-tuple-element.29), channel_id=1, source_target_pairs={{0,1},{1,0},{2,3},{3,2},{4,5},{5,4},{6,7},{7,6},{8,9},{9,8},{10,11... | collective-permute-start | bytes 1572872 | tf_op jit(solution)/shard_map/ppermute | solution.py:241
  116.2 13.0 %collective-permute-start.9 = (bf16[128,2048]{1,0:T(8,128)(2,1)}, bf16[128,2048]{1,0:T(8,128)(2,1)S(1)}, u32[]{:S(2)}, u32[]{:S(2)}) collective-permute-start(bf16[128,2048]{1,0:T(8,128)(2,1)} %get-tuple-element.27), channel_id=1, source_target_pairs={{0,1},{1,0},{2,3},{3,2},{4,5},{5,4},{6,7},{7,6},{8,9},{9,8},{10,11... | collective-permute-start | bytes 1572872 | tf_op jit(solution)/shard_map/ppermute | solution.py:241
  120.7 26.7 %all-to-all-start.3 = ((bf16[8,48,1024]{2,1,0:T(8,128)(2,1)}), bf16[8,48,1024]{2,1,0:T(8,128)(2,1)S(1)}, u32[]{:S(2)}, u32[]{:S(2)}) async-start(bf16[8,48,1024]{2,1,0:T(8,128)(2,1)} %bitcast.30), calls=%async_computation.3 | async-start | bytes 1572864 | tf_op jit(solution)/shard_map/all_to_all | solution.py:367
  126.9 13.9 %copy-start.7 = (bf16[128,2048]{1,0:T(8,128)(2,1)S(1)}, bf16[128,2048]{1,0:T(8,128)(2,1)}, u32[]{:S(2)}) copy-start(bf16[128,2048]{1,0:T(8,128)(2,1)} %get-tuple-element.26) | copy-start | bytes 1572868
  126.9 13.9 %collective-permute-start.11 = (bf16[128,2048]{1,0:T(8,128)(2,1)S(1)}, bf16[128,2048]{1,0:T(8,128)(2,1)S(1)}, u32[]{:S(2)}, u32[]{:S(2)}) collective-permute-start(bf16[128,2048]{1,0:T(8,128)(2,1)S(1)} %add_convert_fusion.1), channel_id=1, source_target_pairs={{0,2},{1,3},{2,0},{3,1},{4,6},{5,7},{6,4},{7,5},{8,10},{9,11},{10,... | collective-permute-start | bytes 1572872 | tf_op jit(solution)/shard_map/ppermute | solution.py:241
  128.8 18.5 %copy-start.10 = (bf16[384,128]{1,0:T(8,128)(2,1)S(1)}, bf16[384,128]{1,0:T(8,128)(2,1)}, u32[]{:S(2)}) copy-start(bf16[384,128]{1,0:T(8,128)(2,1)} %get-tuple-element.31) | copy-start | bytes 294916
  (6 other events, 22.2 us)
